TPU v7x, 32 devices: a whole 2x2x4 slice. The times are simulated.
32 devices in a mesh: grp: 2 (over x), ep: 8 (over z, y), tp: 2 (over core).
Axes of the slice: x: 2, y: 2, z: 4, core: 2. Of those that a mesh axis runs over, the one named last changes fastest.
Arguments:
- tokens: bfloat16 [8192, 2048], P(('grp', 'ep', 'tp')), parts along dimension 0, may hold values from -6 to 6
- norm_gain: float32 [2048], replicated, may hold values from 0.1 to 1.9
- expert_ids: int32 [8192, 4], P(('grp', 'ep', 'tp')), parts along dimension 0, may hold values from 0 to 31, all different within a row; in each aligned block of 256 rows (0 to 255, 256 to 511, ...) at most 40 rows name the same one
- gate_weights: float32 [8192, 4], P(('grp', 'ep', 'tp')), parts along dimension 0, may hold values from 0.1 to 1
- expert_gate: bfloat16 [32, 2048, 512], P('ep', None, 'tp'), may hold values from -0.125 to 0.125
- expert_up: bfloat16 [32, 2048, 512], P('ep', None, 'tp'), may hold values from -0.125 to 0.125
- expert_down: bfloat16 [32, 512, 2048], P('ep', 'tp'), may hold values from -0.25 to 0.25
- shared_gate: bfloat16 [2048, 512], replicated, may hold values from -0.125 to 0.125
- shared_up: bfloat16 [2048, 512], replicated, may hold values from -0.125 to 0.125
- shared_down: bfloat16 [512, 2048], replicated, may hold values from -0.25 to 0.25
- post_gain: float32 [2048], replicated, may hold values from 0.1 to 1.9
Outputs:
- mixed: bfloat16 [8192, 2048], P(('grp', 'ep', 'tp')), parts along dimension 0
There are 2 independent parts, one for each index of `grp`. A program takes and returns all parts, laid end to end along the dimension named above; an argument that names none is the same for every part. Nothing has to cross between parts.
Inputs may be any that keep to these rules, and one draw needn't show every extreme that they name: `expert_ids`: each row names 4 different experts; in each device's aligned block of 256 rows no expert is named by more than 40 rows, a bound that some block reaches.
All inputs are finite; a program needn't handle non-finite values.
Results may differ from a plain program's by a relative error of at most 0.0067.
Values may be sent and summed in bfloat16 or wider, within the bound.
A program may use at most 128 MiB of HBM per device.

v0:
```python
import functools

import jax
import jax.numpy as jnp
from jax import lax
from jax.experimental import pallas as pl
from jax.experimental.pallas import tpu as pltpu
from jax.sharding import PartitionSpec as P

EXPERTS = 32
CAP = 40


EPS = 1e-06


def rms_scale(inputs, gain):
    mean_sq = jnp.mean(inputs * inputs, axis=-1, keepdims=True)
    return inputs * lax.rsqrt(mean_sq + EPS) * gain


def expert_rows(tok_rows, w_gate, w_up, w_down):
    gate_act = jnp.einsum("erd,edf->erf", tok_rows, w_gate, preferred_element_type=jnp.float32)
    up_act = jnp.einsum("erd,edf->erf", tok_rows, w_up, preferred_element_type=jnp.float32)
    hidden = (jax.nn.silu(gate_act) * up_act).astype(jnp.bfloat16)
    return jnp.einsum("erf,efd->erd", hidden, w_down, preferred_element_type=jnp.float32)


def shared_branch(normed, shared_gate, shared_up, shared_down):
    shared_act = jnp.dot(normed, shared_gate, preferred_element_type=jnp.float32)
    shared_lift = jnp.dot(normed, shared_up, preferred_element_type=jnp.float32)
    shared_hidden = (jax.nn.silu(shared_act) * shared_lift).astype(jnp.bfloat16)
    return jnp.dot(shared_hidden, shared_down, preferred_element_type=jnp.float32)


def body(
    tokens,
    norm_gain,
    expert_ids,
    gate_weights,
    expert_gate,
    expert_up,
    expert_down,
    shared_gate,
    shared_up,
    shared_down,
    post_gain,
):
    tok_count = tokens.shape[0]
    top_count = expert_ids.shape[1]
    width = tokens.shape[1]
    normed = rms_scale(tokens.astype(jnp.float32), norm_gain).astype(jnp.bfloat16)
    flat_ids = expert_ids.reshape(-1)
    onehot = (flat_ids[:, None] == jnp.arange(EXPERTS, dtype=jnp.int32)[None, :]).astype(jnp.int32)
    slot_index = jnp.sum(jnp.cumsum(onehot, axis=0) * onehot, axis=1) - 1
    position = flat_ids * CAP + slot_index
    source_row = jnp.arange(tok_count * top_count, dtype=jnp.int32) // top_count
    lookup = jnp.full((EXPERTS * CAP,), tok_count, jnp.int32).at[position].set(source_row)
    padded = jnp.concatenate([normed, jnp.zeros((1, width), jnp.bfloat16)], axis=0)
    outgoing = padded[lookup].reshape(EXPERTS, 1, CAP, width)
    whole_gate, whole_up, whole_down = (
        lax.all_gather(expert_gate, "tp", axis=2, tiled=True),
        lax.all_gather(expert_up, "tp", axis=2, tiled=True),
        lax.all_gather(expert_down, "tp", axis=1, tiled=True),
    )
    arrived = lax.all_to_all(outgoing, "ep", split_axis=0, concat_axis=1, tiled=True)
    local_experts = arrived.shape[0]
    senders = arrived.shape[1]
    slots = arrived.shape[2]
    tok_rows = arrived.reshape(local_experts, senders * slots, width)
    result = expert_rows(tok_rows, whole_gate, whole_up, whole_down).astype(jnp.bfloat16)
    result = result.reshape(local_experts, senders, slots, width)
    returned = lax.all_to_all(result, "ep", split_axis=1, concat_axis=0, tiled=True)
    shared_out = shared_branch(normed, shared_gate, shared_up, shared_down)
    back_rows = returned.reshape(EXPERTS * CAP, width)
    picked = back_rows[position].reshape(tok_count, top_count, width).astype(jnp.float32)
    routed = jnp.einsum("tk,tkd->td", gate_weights, picked)
    combined = routed + shared_out
    return rms_scale(combined, post_gain).astype(jnp.bfloat16)

VMEM_ALL = 67043328
MESH = pl.DeviceIdType.MESH


def ring_bytes(shapes):
    total = 0
    for shape, kind in shapes:
        count = jnp.dtype(kind).itemsize
        for size in shape:
            count *= size
        total += count
    return total


ROLES = ("tokens", "shared", "expert", "give", "total", "finish", "weights", "own")
TOKENS_AT, SHARED_AT, EXPERT_AT, GIVE_AT, TOTAL_AT, FINISH_AT, WEIGHTS_AT, OWN_AT = range(8)


def plain_order(nz, chunks, z):
    near = sorted(range(nz), key=lambda s: (abs(s - z), s))
    far = sorted((s for s in range(nz) if s != z), key=lambda s: (-abs(s - z), s)) + [z]
    steps = [(OWN_AT, z, c) for c in range(chunks)] if 0 < z < nz - 1 else []
    steps += [(TOKENS_AT, z, c) for c in range(chunks)] + [(SHARED_AT, z, 0)]
    steps += [(TOKENS_AT, s, c) for s in near[1:2] for c in range(chunks)] + [(WEIGHTS_AT, z, 0)]
    for k, s in enumerate(near):
        steps += [(EXPERT_AT, s, c) for c in range(chunks)]
        if s != z:
            steps += [(GIVE_AT, s, c) for c in range(chunks)]
        steps += [(TOKENS_AT, q, c) for q in near[k + 2 : k + 3] for c in range(chunks)]
    steps += [(GIVE_AT, z, c) for c in range(chunks)]
    steps += [(TOTAL_AT, s, c) for s in far for c in range(chunks)]
    return steps + [(FINISH_AT, z, 0)]


def step_tables(nz, chunks, z):
    orders = [ORDERS(nz, chunks, q) for q in range(nz)]
    length = max(len(order) for order in orders)
    size = len(ROLES) * nz * chunks + 1
    per = 1
    while size ** (per + 1) < 1 << 31:
        per += 1
    count = -(-length // per)
    packed = []
    for order in orders:
        flat = [(role * nz + s) * chunks + c for role, s, c in order]
        flat += [size - 1] * (count * per - len(flat))
        packed.append([sum(v * size**i for i, v in enumerate(flat[k * per : (k + 1) * per])) for k in range(count)])

    def step_of(k):
        group, inside = k // per, k % per
        row = []
        for i in range(count):
            value = jnp.int32(packed[0][i])
            for q in range(1, nz):
                value = jnp.where(z == q, packed[q][i], value)
            row.append(value)
        bit = 1
        while len(row) > 1:
            odd = group // bit % 2 == 1
            row = [jnp.where(odd, row[i + 1], row[i]) if i + 1 < len(row) else row[i] for i in range(0, len(row), 2)]
            bit *= 2
        code = row[0]
        for i in range(per - 1):
            code = jnp.where(inside > i, code // size, code)
        code = code % size
        return code // (nz * chunks), code // chunks % nz, code % chunks

    return length, step_of


def grid_kernel(
    nz,
    top,
    chunks,
    tok_ref,
    ids_ref,
    weights_ref,
    ngain_ref,
    pgain_ref,
    eg_hbm,
    eu_hbm,
    ed_hbm,
    sg_hbm,
    su_hbm,
    sd_hbm,
    out_ref,
    wg,
    wu,
    wd,
    sg,
    su,
    sd,
    blk,
    xa,
    xb,
    xcat,
    gate_sum,
    up_sum,
    yout,
    back,
    mine,
    pick_own,
    pick_par,
    put_own,
    put_par,
    scale,
    meta_a,
    meta_b,
    rs_in,
    shared,
    hid,
    hidden,
    acc,
    load_sem,
    w_send,
    w_recv,
    ag_send,
    ag_recv,
    mt_send,
    mt_recv,
    mb_send,
    mb_recv,
    d_send,
    d_recv,
    r_send,
    r_recv,
    rs_send,
    rs_recv,
):
    rows, width = tok_ref.shape
    experts = eg_hbm.shape[0]
    fh = eg_hbm.shape[2]
    fs = sg.shape[1]
    cw = width // chunks
    slots = experts * CAP
    step_rows = 32
    ep = lax.axis_index("ep")
    tp = lax.axis_index("tp")
    z, y = ep // 2, ep % 2
    par = ep + 1 - 2 * y
    above, below = z < nz - 1, z > 0
    up, dn = jnp.minimum(ep + 2, 2 * nz - 1), jnp.maximum(ep - 2, 0)
    partner = 1 - tp

    barrier = pltpu.get_barrier_semaphore()
    pl.semaphore_signal(barrier, inc=1, device_id={"ep": par}, device_id_type=MESH)
    pl.semaphore_signal(barrier, inc=1, device_id={"tp": partner}, device_id_type=MESH)

    @pl.when(above)
    def _():
        pl.semaphore_signal(barrier, inc=1, device_id={"ep": up}, device_id_type=MESH)

    @pl.when(below)
    def _():
        pl.semaphore_signal(barrier, inc=1, device_id={"ep": dn}, device_id_type=MESH)

    loads = [
        pltpu.make_async_copy(src, dst, load_sem.at[k])
        for k, (src, dst) in enumerate(
            (
                (sg_hbm, sg),
                (su_hbm, su),
                (sd_hbm, sd),
                (eg_hbm, wg.at[0]),
                (eu_hbm, wu.at[0]),
                (ed_hbm, wd.at[0]),
            )
        )
    ]
    for load in loads:
        load.start()

    @pl.loop(0, rows // step_rows)
    def _(r):
        at = pl.ds(pl.multiple_of(r * step_rows, step_rows), step_rows)
        v = rms_scale(tok_ref[at, :].astype(jnp.float32), ngain_ref[...]).astype(jnp.bfloat16)
        for c in range(chunks):
            blk[z, c, at, :] = v[:, c * cw : (c + 1) * cw]

    def remote(src, dst, send, recv, ep_to):
        return pltpu.make_async_remote_copy(
            src_ref=src,
            dst_ref=dst,
            send_sem=send,
            recv_sem=recv,
            device_id={"ep": ep_to},
            device_id_type=MESH,
        )

    def token_copy(way, s, c):
        return remote(blk.at[s, c], blk.at[s, c], ag_send.at[way, s, c], ag_recv.at[s, c], (up, dn)[way])

    def meta_copy(way, s):
        return remote(meta_a.at[s], meta_a.at[s], mt_send.at[way, s], mt_recv.at[s], (up, dn)[way])

    def meta_across(s):
        return remote(meta_a.at[s], meta_b.at[s], mb_send.at[s], mb_recv.at[s], par)

    def give_rows(s, c):
        return remote(yout.at[s, c], xb.at[s, c], d_send.at[s, c], d_recv.at[s, c], par)

    def give_back(s, c):
        return remote(yout.at[s, c], back.at[s, c], r_send.at[s, c], r_recv.at[s, c], par)

    def sum_copy(way, s, c, slot):
        return remote(blk.at[s, c], rs_in.at[slot, c], rs_send.at[s, c], rs_recv.at[slot, c], (up, dn)[way])

    pl.semaphore_wait(barrier, 2 + above.astype(jnp.int32) + below.astype(jnp.int32))

    low = 2 * z < nz
    for way, there, early in ((0, above, low), (1, below, ~low)):

        @pl.when(there & (early | ~above | ~below))
        def _():
            token_copy(way, z, 0).start()

    total_experts = 2 * nz * experts
    ids, weights = ids_ref[...].astype(jnp.float32), weights_ref[...]
    names = lax.broadcasted_iota(jnp.int32, (total_experts, rows), 0).astype(jnp.float32)
    named = jnp.zeros((total_experts, rows), jnp.float32)
    for k in range(top):
        named = jnp.where(ids[k : k + 1] == names, 1.0, named)
    before = lax.broadcasted_iota(jnp.int32, (rows, rows), 0) < lax.broadcasted_iota(jnp.int32, (rows, rows), 1)
    before = jnp.where(before, 1.0, 0.0).astype(jnp.bfloat16)
    rank = jnp.dot(named.astype(jnp.bfloat16), before, preferred_element_type=jnp.float32)
    for k in range(top):
        found = jnp.sum(jnp.where(ids[k : k + 1] == names, rank, 0.0), axis=0, keepdims=True)
        meta_a[z, k : k + 1, :] = ids[k : k + 1] * CAP + found
    meta_a[z, top : 2 * top, :] = weights

    for way, there in enumerate((above, below)):

        @pl.when(there)
        def _():
            meta_copy(way, z).start()

    for way, there, early in ((0, above, low), (1, below, ~low)):

        @pl.when(there & (early | ~above | ~below))
        def _():
            @pl.loop(1, chunks)
            def _(c):
                token_copy(way, z, c).start()

    swaps = [
        pltpu.make_async_remote_copy(
            src_ref=src,
            dst_ref=dst.at[1],
            send_sem=w_send.at[k],
            recv_sem=w_recv.at[k],
            device_id={"tp": partner},
            device_id_type=MESH,
        )
        for k, (src, dst) in enumerate(((eg_hbm, wg), (eu_hbm, wu), (ed_hbm, wd)))
    ]

    for swap in swaps:
        swap.start()

    def own_tokens(c):
        @pl.when(low)
        def _():
            token_copy(1, z, c).start()

        @pl.when(~low)
        def _():
            token_copy(0, z, c).start()

    def pick_table(table, owner):
        want = lax.broadcasted_iota(jnp.int32, (slots, rows), 0).astype(jnp.float32)
        want = want + (owner * slots).astype(jnp.float32)
        hits = [table[k : k + 1] == want for k in range(top)]
        mass = jnp.zeros((slots, rows), jnp.float32)
        for k in range(top):
            mass = jnp.where(hits[k], table[top + k : top + k + 1], mass)
        pick = functools.reduce(jnp.logical_or, hits)
        return jnp.where(pick, 1.0, 0.0).astype(jnp.bfloat16), jnp.sum(mass, axis=1, keepdims=True)

    def put_table(turned, owner):
        want = lax.broadcasted_iota(jnp.int32, (rows, slots), 1).astype(jnp.float32)
        want = want + (owner * slots).astype(jnp.float32)
        pick = functools.reduce(jnp.logical_or, [turned[:, k : k + 1] == want for k in range(top)])
        return jnp.where(pick, 1.0, 0.0).astype(jnp.bfloat16)

    def spread(column):
        return jnp.broadcast_to(column, (slots, 128)).reshape(experts, CAP, 128)

    def take_meta(s):
        @pl.when(s != z)
        def _():
            meta_copy(0, s).wait_recv()

        @pl.when((s < z) & above)
        def _():
            meta_copy(0, s).start()

        @pl.when((s > z) & below)
        def _():
            meta_copy(1, s).start()

        meta_across(s).start()
        table = meta_a[s]
        pick, mass = pick_table(table, ep)
        pick_own[s] = pick
        scale[s, :, :CAP, :] = spread(mass)
        pick_par[s] = pick_table(table, par)[0]
        turned = table.T
        put_own[s] = put_table(turned, ep)
        put_par[s] = put_table(turned, par)

    def take_tokens(s, c):
        @pl.when(s != z)
        def _():
            token_copy(0, s, c).wait_recv()

        @pl.when((s < z) & above)
        def _():
            token_copy(0, s, c).start()

        @pl.when((s > z) & below)
        def _():
            token_copy(1, s, c).start()

        @pl.when(c == 0)
        def _():
            take_meta(s)

        there = jnp.dot(pick_par[s], blk[s, c], preferred_element_type=jnp.float32)
        yout[s, c] = there.astype(jnp.bfloat16)
        give_rows(s, c).start()
        here = jnp.dot(pick_own[s], blk[s, c], preferred_element_type=jnp.float32)
        xa[s, c] = here.astype(jnp.bfloat16)

    tile = min(256, fs)

    def shared_expert():
        for load in loads[:3]:
            load.wait()

        @pl.loop(0, fs // tile)
        def _(k):
            at = pl.ds(pl.multiple_of(k * tile, tile), tile)
            x = jnp.concatenate([blk[z, c] for c in range(chunks)], axis=1)
            g = jnp.dot(x, sg[:, at], preferred_element_type=jnp.float32)
            u = jnp.dot(x, su[:, at], preferred_element_type=jnp.float32)
            hid[:, at] = (jax.nn.silu(g) * u).astype(jnp.bfloat16)

        @pl.loop(0, chunks)
        def _(c):
            at = pl.ds(pl.multiple_of(c * cw, cw), cw)
            shared[c] = jnp.dot(hid[...], sd[:, at], preferred_element_type=jnp.float32)

    def weights_here():
        for load in loads[3:]:
            load.wait()
        for swap in swaps:
            swap.wait_recv()

    gate_sum[...] = jnp.zeros_like(gate_sum)
    up_sum[...] = jnp.zeros_like(up_sum)

    def expert(s, c):
        @pl.when(c == 0)
        def _():
            meta_across(s).wait_recv()
            scale[s, :, CAP:, :] = spread(pick_table(meta_b[s], ep)[1])

        give_rows(s, c).wait_recv()
        depth = pl.ds(pl.multiple_of(c * cw, cw), cw)
        for e in range(experts):
            xcat[e, :CAP, :] = xa[s, c, e * CAP : (e + 1) * CAP, :]
            xcat[e, CAP:, :] = xb[s, c, e * CAP : (e + 1) * CAP, :]
        for e in range(experts):
            for h in range(2):
                gate_sum[h, e] += jnp.dot(xcat[e], wg[h, e, depth, :], preferred_element_type=jnp.float32)
                up_sum[h, e] += jnp.dot(xcat[e], wu[h, e, depth, :], preferred_element_type=jnp.float32)

        @pl.when(c == chunks - 1)
        def _():
            @pl.loop(0, experts)
            def _(e):
                weight = scale[s, e][:, :1]
                for h in range(2):
                    g, u = gate_sum[h, e], up_sum[h, e]
                    hidden[s, h, e] = (jax.nn.silu(g) * u * weight).astype(jnp.bfloat16)
                    gate_sum[h, e] = jnp.zeros_like(g)
                    up_sum[h, e] = jnp.zeros_like(u)

    def give(s, c):
        give_rows(s, c).wait_send()
        at = pl.ds(pl.multiple_of(c * cw, cw), cw)
        for e in range(experts):
            down = jnp.dot(hidden[s, 0, e], wd[0, e, :, at], preferred_element_type=jnp.float32)
            down += jnp.dot(hidden[s, 1, e], wd[1, e, :, at], preferred_element_type=jnp.float32)
            down = down.astype(jnp.bfloat16)
            yout[s, c, e * CAP : (e + 1) * CAP, :] = down[CAP:]
            mine[s, c, e * CAP : (e + 1) * CAP, :] = down[:CAP]
        give_back(s, c).start()

    def total(s, c):
        give_back(s, c).wait_recv()
        own = jnp.dot(put_own[s], mine[s, c], preferred_element_type=jnp.float32)
        own += jnp.dot(put_par[s], back[s, c], preferred_element_type=jnp.float32)
        acc[...] = own

        @pl.when((s >= z) & below)
        def _():
            sum_copy(0, s, c, s).wait_recv()
            acc[...] += rs_in[s, c].astype(jnp.float32)

        @pl.when((s <= z) & above)
        def _():
            slot = jnp.where(s == z, nz, s)
            sum_copy(1, s, c, slot).wait_recv()
            acc[...] += rs_in[slot, c].astype(jnp.float32)

        @pl.when((s < z) & above)
        def _():
            token_copy(0, s, c).wait_send()

        @pl.when((s > z) & below)
        def _():
            token_copy(1, s, c).wait_send()

        @pl.when(s == z)
        def _():
            shared[c] += acc[...]

        @pl.when(s != z)
        def _():
            blk[s, c] = acc[...].astype(jnp.bfloat16)

        @pl.when(s > z)
        def _():
            sum_copy(0, s, c, s).start()

        @pl.when(s < z)
        def _():
            sum_copy(1, s, c, jnp.where(s == z - 1, nz, s)).start()

    def finish():
        @pl.loop(0, rows // step_rows)
        def _(r):
            at = pl.ds(pl.multiple_of(r * step_rows, step_rows), step_rows)
            both = jnp.concatenate([shared[c, at, :] for c in range(chunks)], axis=1)
            out_ref[at, :] = rms_scale(both, pgain_ref[...]).astype(jnp.bfloat16)

    length, step_of = step_tables(nz, chunks, z)

    @pl.loop(0, length)
    def _(k):
        role, s, c = step_of(k)
        pl.when(role == TOKENS_AT)(lambda: take_tokens(s, c))
        pl.when(role == SHARED_AT)(shared_expert)
        pl.when(role == EXPERT_AT)(lambda: expert(s, c))
        pl.when(role == GIVE_AT)(lambda: give(s, c))
        pl.when(role == TOTAL_AT)(lambda: total(s, c))
        pl.when(role == FINISH_AT)(finish)
        pl.when(role == WEIGHTS_AT)(weights_here)
        pl.when(role == OWN_AT)(lambda: own_tokens(c))

    for swap in swaps:
        swap.wait_send()
    for way, there in enumerate((above, below)):

        @pl.when(there)
        def _():
            meta_copy(way, z).wait_send()

            @pl.loop(0, chunks)
            def _(c):
                token_copy(way, z, c).wait_send()

    @pl.loop(0, nz)
    def _(s):
        @pl.when((s < z) & above)
        def _():
            meta_copy(0, s).wait_send()

        @pl.when((s > z) & below)
        def _():
            meta_copy(1, s).wait_send()

        meta_across(s).wait_send()

        @pl.loop(0, chunks)
        def _(c):
            give_back(s, c).wait_send()

            @pl.when(s != z)
            def _():
                sum_copy(0, s, c, s).wait_send()


def grid_shapes(nz, chunks, rows, width, meta_rows, eg, ed, sg, sd):
    bf, f32 = jnp.bfloat16, jnp.float32
    experts = eg.shape[0]
    fs = sg.shape[1]
    cw = width // chunks
    slots = experts * CAP
    return [
        ((2,) + eg.shape, bf),
        ((2,) + eg.shape, bf),
        ((2,) + ed.shape, bf),
        (sg.shape, bf),
        (sg.shape, bf),
        (sd.shape, bf),
        ((nz, chunks, rows, cw), bf),
        ((nz, chunks, slots, cw), bf),
        ((nz, chunks, slots, cw), bf),
        ((experts, 2 * CAP, cw), bf),
        ((2, experts, 2 * CAP, eg.shape[2]), f32),
        ((2, experts, 2 * CAP, eg.shape[2]), f32),
        ((nz, chunks, slots, cw), bf),
        ((nz, chunks, slots, cw), bf),
        ((nz, chunks, slots, cw), bf),
        ((nz, slots, rows), bf),
        ((nz, slots, rows), bf),
        ((nz, rows, slots), bf),
        ((nz, rows, slots), bf),
        ((nz, experts, 2 * CAP, 128), f32),
        ((nz, meta_rows, rows), f32),
        ((nz, meta_rows, rows), f32),
        ((nz + 1, chunks, rows, cw), bf),
        ((chunks, rows, cw), f32),
        ((rows, fs), bf),
        ((nz, 2, experts, 2 * CAP, eg.shape[2]), bf),
        ((rows, cw), f32),
    ]


def grid_body(
    n,
    tokens,
    norm_gain,
    expert_ids,
    gate_weights,
    expert_gate,
    expert_up,
    expert_down,
    shared_gate,
    shared_up,
    shared_down,
    post_gain,
):
    rows, width = tokens.shape
    top = expert_ids.shape[1]
    nz = n // 2
    chunks = CHUNKS
    meta_rows = -(-2 * top // 8) * 8
    shapes = grid_shapes(nz, chunks, rows, width, meta_rows, expert_gate, expert_down, shared_gate, shared_down)
    if ring_bytes(shapes) + 4 * rows * width > VMEM_ALL - (2 << 20):
        return body(
            tokens,
            norm_gain,
            expert_ids,
            gate_weights,
            expert_gate,
            expert_up,
            expert_down,
            shared_gate,
            shared_up,
            shared_down,
            post_gain,
        )
    dma = pltpu.SemaphoreType.DMA
    vmem = pl.BlockSpec(memory_space=pltpu.VMEM)
    hbm = pl.BlockSpec(memory_space=pl.ANY)
    return pl.pallas_call(
        functools.partial(grid_kernel, nz, top, chunks),
        out_shape=jax.ShapeDtypeStruct((rows, width), jnp.bfloat16),
        in_specs=[vmem] * 5 + [hbm] * 6,
        out_specs=vmem,
        scratch_shapes=[pltpu.VMEM(shape, kind) for shape, kind in shapes]
        + [
            dma((6,)),
            dma((3,)),
            dma((3,)),
            dma((2, nz, chunks)),
            dma((nz, chunks)),
            dma((2, nz)),
            dma((nz,)),
            dma((nz,)),
            dma((nz,)),
            dma((nz, chunks)),
            dma((nz, chunks)),
            dma((nz, chunks)),
            dma((nz, chunks)),
            dma((nz, chunks)),
            dma((nz + 1, chunks)),
        ],
        compiler_params=pltpu.CompilerParams(
            collective_id=0, has_side_effects=True, vmem_limit_bytes=VMEM_ALL
        ),
    )(
        tokens,
        expert_ids.T,
        gate_weights.T,
        norm_gain.reshape(1, width),
        post_gain.reshape(1, width),
        expert_gate,
        expert_up,
        expert_down,
        shared_gate,
        shared_up,
        shared_down,
    )


CHUNKS = 4
STEPS = (
    (
        0, 3, 2, 1, 10, 100, 20, 21, 600, 22, 220, 221, 23, 222, 30, 223,
        323, 320, 321, 200, 201, 31, 423, 33, 420, 421, 32, 202, 203, 322, 12, 230,
        231, 232, 233, 333, 422, 331, 332, 11, 433, 210, 431, 13, 330, 211, 432, 212,
        213, 311, 430, 312, 310, 411, 313, 303, 412, 301, 413, 302, 410, 300, 402, 403,
        401, 400, 500,
    ),
    (
        10, 710, 12, 11, 20, 0, 21, 13, 22, 23, 110, 1, 30, 610, 3, 31,
        220, 33, 221, 2, 222, 32, 223, 200, 201, 712, 323, 320, 202, 203, 711, 321,
        230, 713, 423, 231, 232, 322, 420, 233, 210, 211, 330, 333, 332, 421, 331, 212,
        213, 422, 303, 302, 301, 311, 300, 433, 431, 312, 403, 310, 432, 313, 430, 401,
        402, 411, 412, 400, 413, 410, 510,
    ),
)


def ORDERS(nz, chunks, z):
    if nz != 2 * len(STEPS):
        return plain_order(nz, chunks, z)
    near = min(z, nz - 1 - z)
    steps = [(k // 100, k // 10 % 10, k % 10) for k in STEPS[near]]
    return [(role, s if near == z else nz - 1 - s, c) for role, s, c in steps]


def solution(mesh):
    ringed = mesh.shape["tp"] == 2 and mesh.shape["ep"] % 2 == 0 and mesh.shape["ep"] > 2
    return jax.shard_map(
        functools.partial(grid_body, mesh.shape["ep"]) if ringed else body,
        mesh=mesh,
        in_specs=(
            P(("grp", "ep", "tp"), None),
            P(),
            P(("grp", "ep", "tp"), None),
            P(("grp", "ep", "tp"), None),
            P("ep", None, "tp"),
            P("ep", None, "tp"),
            P("ep", "tp", None),
            P(),
            P(),
            P(),
            P(),
        ),
        out_specs=P(("grp", "ep", "tp"), None),
        check_vma=False,
    )
```

profile of v0, /device:TPU:0, one launch (start us, length us, event | category | flops | bytes accessed | tf_op | source)
XLA Modules:
  0.0 131.4 jit_solution(2828126202328136457)
XLA Ops:
  0.0 129.1 %shard_map.109 = bf16[256,2048]{1,0:T(8,128)(2,1)} custom-call(bf16[256,2048]{1,0:T(8,128)(2,1)} %tok_ref.1, s32[4,256]{1,0:T(4,128)} %bitcast.6, f32[4,256]{1,0:T(4,128)} %bitcast.7, f32[1,2048]{1,0:T(1,128)} %bitcast.4, f32[1,2048]{1,0:T(1,128)} %bitcast.5, bf16[4,2048,256]{2,1,0:T(8,128)(2,1)} %eg_hbm.1, bf16[4,2048,256]{2,1,0:T(8,128)(2,1)} %eu_hbm.1, ...), custom_call_target="tpu_custom_call" | custom-call | tf_op jit(solution)/shard_map/pallas_call | solution.py:649
  129.1 2.3 %copy.13 = bf16[256,2048]{1,0:T(8,128)(2,1)} copy(bf16[256,2048]{1,0:T(8,128)(2,1)} %shard_map.109) | data formatting | bytes 2097152
where the time goes:
time: 132 us; the launch traced here: 131 us
  Pallas kernels  129 us (98%)
  local copies, waits for them, and re-layouts  2.3 us (2%)
    pallas_call x1, Pallas kernels, grid_body(): pl.pallas_call(functools.partial(grid_kernel, nz, top, chunks), out_shape...  129 us

commit v1 on v0

--- a/solution.py
+++ b/solution.py
@@ -287,6 +287,20 @@
 
     pl.semaphore_wait(barrier, 2 + above.astype(jnp.int32) + below.astype(jnp.int32))
 
+    swaps = [
+        pltpu.make_async_remote_copy(
+            src_ref=src,
+            dst_ref=dst.at[1],
+            send_sem=w_send.at[k],
+            recv_sem=w_recv.at[k],
+            device_id={"tp": partner},
+            device_id_type=MESH,
+        )
+        for k, (src, dst) in enumerate(((eg_hbm, wg), (eu_hbm, wu), (ed_hbm, wd)))
+    ]
+    for swap in swaps:
+        swap.start()
+
     low = 2 * z < nz
     for way, there, early in ((0, above, low), (1, below, ~low)):
 
@@ -322,20 +336,6 @@
             def _(c):
                 token_copy(way, z, c).start()
 
-    swaps = [
-        pltpu.make_async_remote_copy(
-            src_ref=src,
-            dst_ref=dst.at[1],
-            send_sem=w_send.at[k],
-            recv_sem=w_recv.at[k],
-            device_id={"tp": partner},
-            device_id_type=MESH,
-        )
-        for k, (src, dst) in enumerate(((eg_hbm, wg), (eu_hbm, wu), (ed_hbm, wd)))
-    ]
-
-    for swap in swaps:
-        swap.start()
 
     def own_tokens(c):
         @pl.when(low)

time: 132 us -> 132 us (level)
  no operation moved by 1% of the time
where the time goes in v1:
time: 132 us; the launch traced here: 131 us
  Pallas kernels  129 us (98%)
  local copies, waits for them, and re-layouts  2.3 us (2%)
    pallas_call x1, Pallas kernels, grid_body(): pl.pallas_call(functools.partial(grid_kernel, nz, top, chunks), out_shape...  129 us

profile of v1, /device:TPU:0, one launch (start us, length us, event | category | flops | bytes accessed | tf_op | source)
XLA Modules:
  0.0 131.2 jit_solution(3925070952804584998)
XLA Ops:
  0.0 128.9 %shard_map.109 = bf16[256,2048]{1,0:T(8,128)(2,1)} custom-call(bf16[256,2048]{1,0:T(8,128)(2,1)} %tok_ref.1, s32[4,256]{1,0:T(4,128)} %bitcast.6, f32[4,256]{1,0:T(4,128)} %bitcast.7, f32[1,2048]{1,0:T(1,128)} %bitcast.4, f32[1,2048]{1,0:T(1,128)} %bitcast.5, bf16[4,2048,256]{2,1,0:T(8,128)(2,1)} %eg_hbm.1, bf16[4,2048,256]{2,1,0:T(8,128)(2,1)} %eu_hbm.1, ...), custom_call_target="tpu_custom_call" | custom-call | tf_op jit(solution)/shard_map/pallas_call | solution.py:649
  128.9 2.3 %copy.13 = bf16[256,2048]{1,0:T(8,128)(2,1)} copy(bf16[256,2048]{1,0:T(8,128)(2,1)} %shard_map.109) | data formatting | bytes 2097152

commit v2 on v1

--- a/solution.py
+++ b/solution.py
@@ -478,10 +478,9 @@
         give_back(s, c).start()
 
     def total(s, c):
+        acc[...] = jnp.dot(put_own[s], mine[s, c], preferred_element_type=jnp.float32)
         give_back(s, c).wait_recv()
-        own = jnp.dot(put_own[s], mine[s, c], preferred_element_type=jnp.float32)
-        own += jnp.dot(put_par[s], back[s, c], preferred_element_type=jnp.float32)
-        acc[...] = own
+        acc[...] += jnp.dot(put_par[s], back[s, c], preferred_element_type=jnp.float32)
 
         @pl.when((s >= z) & below)
         def _():

time: 132 us -> 131 us (level)
  no operation moved by 1% of the time
where the time goes in v2:
time: 131 us
  Pallas kernels  129 us (98%)
  local copies, waits for them, and re-layouts  2.3 us (2%)
    pallas_call x1, Pallas kernels, grid_body(): pl.pallas_call(functools.partial(grid_kernel, nz, top, chunks), out_shape...  129 us

profile of v2, /device:TPU:0, one launch (start us, length us, event | category | flops | bytes accessed | tf_op | source)
XLA Modules:
  0.0 131.2 jit_solution(15315431638777779699)
XLA Ops:
  0.0 128.9 %shard_map.109 = bf16[256,2048]{1,0:T(8,128)(2,1)} custom-call(bf16[256,2048]{1,0:T(8,128)(2,1)} %tok_ref.1, s32[4,256]{1,0:T(4,128)} %bitcast.6, f32[4,256]{1,0:T(4,128)} %bitcast.7, f32[1,2048]{1,0:T(1,128)} %bitcast.4, f32[1,2048]{1,0:T(1,128)} %bitcast.5, bf16[4,2048,256]{2,1,0:T(8,128)(2,1)} %eg_hbm.1, bf16[4,2048,256]{2,1,0:T(8,128)(2,1)} %eu_hbm.1, ...), custom_call_target="tpu_custom_call" | custom-call | tf_op jit(solution)/shard_map/pallas_call | solution.py:648
  128.9 2.3 %copy.13 = bf16[256,2048]{1,0:T(8,128)(2,1)} copy(bf16[256,2048]{1,0:T(8,128)(2,1)} %shard_map.109) | data formatting | bytes 2097152
